TPU v7x, 32 devices: a whole 2x2x4 slice. The times are simulated.
32 devices in a mesh: sp: 8 (over z, y), tp: 4 (over x, core).
Axes of the slice: x: 2, y: 2, z: 4, core: 2. Of those that a mesh axis runs over, the one named last changes fastest.
Arguments:
- tokens: bfloat16 [6144, 2048], P('sp', 'tp'), may hold values from -12 to 12
- query_weight: bfloat16 [2048, 1024], P('sp', 'tp'), may hold values from -0.176776695 to 0.176776695
- key_projection: bfloat16 [2048, 512], P('sp', 'tp'), may hold values from -0.176776695 to 0.176776695
- value_projection: bfloat16 [2048, 512], P('sp', 'tp'), may hold values from -0.125 to 0.125
- conv_in_weight: bfloat16 [2048, 1024], P('sp', 'tp'), may hold values from -0.125 to 0.125
- conv_gate_out: bfloat16 [2048, 1024], P('sp', 'tp'), may hold values from -0.125 to 0.125
- conv_gate_in: bfloat16 [2048, 1024], P('sp', 'tp'), may hold values from -0.125 to 0.125
- conv_taps: bfloat16 [3, 1024], P(None, 'tp'), may hold values from -3 to 3
- head_sink_logit: float32 [8], P('tp'), may hold values from 3 to 8
- out_attn_weight: bfloat16 [1024, 2048], P('tp', 'sp'), may hold values from -5 to 5
- out_conv_weight: bfloat16 [1024, 2048], P('tp', 'sp'), may hold values from -0.5 to 0.5
- out_gain: float32 [2048], P('tp'), may hold values from 0.1 to 1.9
Outputs:
- mixed: bfloat16 [6144, 2048], P('sp', 'tp')
All inputs are finite; a program needn't handle non-finite values.
Results may differ from a plain program's by a relative error of at most 0.014.
Values may be sent and summed in bfloat16 or wider, within the bound.
A program may use at most 64 MiB of HBM per device.

v0:
```python
import jax
import jax.numpy as jnp
from jax import lax
from jax.sharding import PartitionSpec as P

HEAD_SIZE = 128
WINDOW = 128
GRID = 64


NEG_BIG = -1e30
THETA = 10000.0
EPS = 1e-05


def with_halo(block, sides, width):
    for axis, dim in sides:
        count = lax.axis_size(axis)
        forward = [(i, i + 1) for i in range(count - 1)]
        backward = [(target, source) for source, target in forward]
        low = lax.ppermute(
            lax.slice_in_dim(block, block.shape[dim] - width, None, axis=dim), axis, forward
        )
        high = lax.ppermute(lax.slice_in_dim(block, 0, width, axis=dim), axis, backward)
        block = jnp.concatenate([low, block, high], axis=dim)
    return block


def rope_tables(positions):
    row = (positions // GRID).astype(jnp.float32)
    column = (positions % GRID).astype(jnp.float32)
    half = HEAD_SIZE // 2
    inverse = THETA ** (-jnp.arange(0, half, 2, dtype=jnp.float32) / half)
    angle_row = row[:, None] * inverse
    angle_col = column[:, None] * inverse
    angles = jnp.concatenate([angle_row, angle_row, angle_col, angle_col], -1)
    return (jnp.cos(angles)[:, None, :], jnp.sin(angles)[:, None, :])


def rotate(vectors, cosine, sine):
    first, second, third, fourth = jnp.split(vectors, 4, axis=-1)
    turned = jnp.concatenate([-second, first, -fourth, third], -1)
    return vectors * cosine + turned * sine


def attend(query_vectors, paired, head_sink_logit, offset, total_tokens):
    item_count = query_vectors.shape[0]
    kv_heads = paired.shape[1] // (2 * HEAD_SIZE)
    head_group = query_vectors.shape[1] // (kv_heads * HEAD_SIZE)
    blocks = item_count // WINDOW
    padded = with_halo(paired, (("sp", 0),), WINDOW)
    shaped = padded.reshape(blocks + 2, WINDOW, paired.shape[1])
    banded = jnp.concatenate([shaped[:-2], shaped[1:-1], shaped[2:]], axis=1)
    banded = banded.reshape(blocks, 3 * WINDOW, 2, kv_heads, HEAD_SIZE)
    key_band = banded[:, :, 0]
    value_band = banded[:, :, 1]
    query_blocks = query_vectors.reshape(blocks, WINDOW, kv_heads, head_group, HEAD_SIZE)
    scores = jnp.einsum(
        "nqhgd,nkhd->nhgqk", query_blocks, key_band, preferred_element_type=jnp.float32
    ) * HEAD_SIZE ** (-0.5)
    block_start = offset + jnp.arange(blocks, dtype=jnp.int32)[:, None] * WINDOW
    query_pos = block_start + jnp.arange(WINDOW, dtype=jnp.int32)[None, :]
    key_pos = block_start - WINDOW + jnp.arange(3 * WINDOW, dtype=jnp.int32)[None, :]
    distance = key_pos[:, None, :] - query_pos[:, :, None]
    valid = (
        (jnp.abs(distance) <= WINDOW)
        & (key_pos[:, None, :] >= 0)
        & (key_pos[:, None, :] < total_tokens)
    )
    scores = jnp.where(valid[:, None, None], scores, NEG_BIG)
    sink_col = head_sink_logit.reshape(1, kv_heads, head_group, 1, 1)
    top = jnp.maximum(jnp.max(scores, -1, keepdims=True), sink_col)
    weights = jnp.exp(scores - top)
    denominator = jnp.sum(weights, -1, keepdims=True) + jnp.exp(sink_col - top)
    probs = (weights / denominator).astype(jnp.bfloat16)
    mixed_heads = jnp.einsum(
        "nhgqk,nkhd->nqhgd", probs, value_band, preferred_element_type=jnp.float32
    )
    return mixed_heads.reshape(item_count, kv_heads * head_group * HEAD_SIZE).astype(jnp.bfloat16)


def convolve(gate_before, conv_input, gate_after, conv_taps):
    sectioned = (gate_before * conv_input).astype(jnp.bfloat16)
    bordered = with_halo(sectioned, (("sp", 0),), 1)
    taps = conv_taps.astype(jnp.float32)
    conv_mix = bordered[:-2] * taps[0] + bordered[1:-1] * taps[1] + bordered[2:] * taps[2]
    return (gate_after * conv_mix).astype(jnp.bfloat16)


def body(
    tokens,
    query_weight,
    key_projection,
    value_projection,
    conv_in_weight,
    conv_gate_out,
    conv_gate_in,
    conv_taps,
    head_sink_logit,
    out_attn_weight,
    out_conv_weight,
    out_gain,
):
    whole = lax.all_gather(tokens, "tp", axis=1, tiled=True)
    item_count = whole.shape[0]
    offset = lax.axis_index("sp") * item_count
    total_tokens = item_count * lax.axis_size("sp")
    positions = offset + jnp.arange(item_count, dtype=jnp.int32)
    cosine, sine = rope_tables(positions)
    pieces = (
        lax.all_gather(query_weight, "sp", axis=0, tiled=True),
        lax.all_gather(key_projection, "sp", axis=0, tiled=True),
        lax.all_gather(value_projection, "sp", axis=0, tiled=True),
        lax.all_gather(conv_in_weight, "sp", axis=0, tiled=True),
        lax.all_gather(conv_gate_out, "sp", axis=0, tiled=True),
        lax.all_gather(conv_gate_in, "sp", axis=0, tiled=True),
    )
    query_raw, key_unrotated, value_raw, conv_input, gate_after, gate_before = tuple(
        (jnp.dot(whole, piece, preferred_element_type=jnp.float32) for piece in pieces)
    )
    query_vectors = (
        rotate(query_raw.reshape(item_count, -1, HEAD_SIZE), cosine, sine)
        .reshape(item_count, -1)
        .astype(jnp.bfloat16)
    )
    key_rows = (
        rotate(key_unrotated.reshape(item_count, -1, HEAD_SIZE), cosine, sine)
        .reshape(item_count, -1)
        .astype(jnp.bfloat16)
    )
    paired = jnp.concatenate([key_rows, value_raw.astype(jnp.bfloat16)], 1)
    attention_out = attend(query_vectors, paired, head_sink_logit, offset, total_tokens)
    conv_out = convolve(gate_before, conv_input, gate_after, conv_taps)
    mixer_rows = jnp.concatenate([attention_out, conv_out], 1)
    stacked = jnp.concatenate([out_attn_weight, out_conv_weight], 0)
    own_width = out_gain.shape[0]
    partial_sums = jnp.dot(
        mixer_rows,
        lax.all_gather(stacked, "sp", axis=1, tiled=True),
        preferred_element_type=jnp.float32,
    )
    summed = lax.psum_scatter(
        partial_sums.astype(jnp.bfloat16), "tp", scatter_dimension=1, tiled=True
    ).astype(jnp.float32)
    full_width = own_width * lax.axis_size("tp")
    first_sum, square_sum = lax.psum((jnp.sum(summed, 1), jnp.sum(summed * summed, 1)), "tp")
    mean = first_sum / full_width
    spread = square_sum / full_width - mean * mean
    normed = (summed - mean[:, None]) * lax.rsqrt(spread[:, None] + EPS) * out_gain
    return normed.astype(jnp.bfloat16)


def solution(mesh):
    return jax.shard_map(
        body,
        mesh=mesh,
        in_specs=(
            P("sp", "tp"),
            P("sp", "tp"),
            P("sp", "tp"),
            P("sp", "tp"),
            P("sp", "tp"),
            P("sp", "tp"),
            P("sp", "tp"),
            P(None, "tp"),
            P("tp"),
            P("tp", "sp"),
            P("tp", "sp"),
            P("tp"),
        ),
        out_specs=P("sp", "tp"),
        check_vma=False,
    )
```

profile of v0, /device:TPU:0, one launch (start us, length us, event | category | flops | bytes accessed | tf_op | source)
XLA Modules:
  0.0 316.7 jit_solution(2554159531670918031)
XLA Ops:
  6.5 0.7 all-gather.7.cloned.1.call-update
  7.3 0.7 all-gather.13.cloned.1.call-update
  8.1 0.7 all-gather.15.cloned.1.call-update
  8.8 0.5 all-gather.9.cloned.1.call-update
  9.4 0.5 all-gather.11.cloned.1.call-update
  10.0 1.7 pad_maximum_fusion.9
  11.9 35.7 %all_gather.25 = bf16[2048,128]{1,0:T(8,128)(2,1)} all-gather(bf16[256,128]{1,0:T(8,128)(2,1)} %param.14), channel_id=1, replica_groups=mesh['sp'=8,'tp'=4] {'sp'}, dimensions={0}, use_global_device_ids=true | all-gather | bytes 589824 | tf_op jit(solution)/shard_map/all_gather | solution.py:112
  47.6 33.9 %all_gather.26 = bf16[2048,128]{1,0:T(8,128)(2,1)} all-gather(bf16[256,128]{1,0:T(8,128)(2,1)S(1)} %copy-done.6), channel_id=1, replica_groups=mesh['sp'=8,'tp'=4] {'sp'}, dimensions={0}, use_global_device_ids=true | all-gather | bytes 589824 | tf_op jit(solution)/shard_map/all_gather | solution.py:113
  81.6 0.1 broadcast_multiply_fusion.1
  81.7 2.8 fusion.10
  84.4 3.3 %fusion.40 = f32[768,128]{0,1:T(8,128)S(1)} fusion(bf16[768,2048]{1,0:T(8,128)(2,1)} %all-gather.7.cloned.1.call-done, bf16[2048,128]{1,0:T(8,128)(2,1)} %all_gather.25), kind=kOutput, calls=%fused_computation.97 | convolution fusion | flops 402653184 | bytes 4063232 | tf_op jit(solution)/shard_map/dot_general | solution.py:119
  87.8 2.4 fusion.21
  90.2 1.2 convolution_convert_fusion.2
  91.4 0.7 fusion.24
  92.1 4.0 %collective-permute-start = (bf16[128,256]{0,1:T(8,128)(2,1)}, bf16[128,256]{0,1:T(8,128)(2,1)}, u32[]{:S(2)}, u32[]{:S(2)}) collective-permute-start(bf16[128,256]{0,1:T(8,128)(2,1)} %get-tuple-element.16), channel_id=1, source_target_pairs={{0,4},{4,8},{8,12},{12,16},{16,20},{20,24},{24,28},{1,5},{5,9},{9,... | collective-permute-start | bytes 196616 | tf_op jit(solution)/shard_map/ppermute | solution.py:21
  96.1 1.3 collective-permute-start.1
  97.4 3.1 fusion.42
  100.5 25.6 %all-gather.15.cloned.1.call-done = bf16[2048,256]{1,0:T(8,128)(2,1)} async-done(((bf16[256,256]{1,0:T(8,128)(2,1)}), bf16[2048,256]{1,0:T(8,128)(2,1)}) %all-gather.15.cloned.1.call-update) | async-done | bytes 1048592 | tf_op jit(solution)/shard_map/all_gather | solution.py:114
  126.1 2.4 fusion.6
  128.5 0.5 fusion.38
  129.1 3.0 collective-permute-start.2
  132.1 1.5 collective-permute-start.3
  133.6 33.5 %all-gather.9.cloned.1.call-done = bf16[2048,256]{1,0:T(8,128)(2,1)} async-done(((bf16[256,256]{1,0:T(8,128)(2,1)}), bf16[2048,256]{1,0:T(8,128)(2,1)}) %all-gather.9.cloned.1.call-update) | async-done | bytes 1048592 | tf_op jit(solution)/shard_map/all_gather | solution.py:111
  167.1 2.3 fusion.41
  169.6 0.8 copy-done.2
  170.4 0.9 fusion.15
  171.3 2.2 reshape.326
  173.6 34.5 %all-gather.11.cloned.1.call-done = bf16[2048,256]{1,0:T(8,128)(2,1)} async-done(((bf16[256,256]{1,0:T(8,128)(2,1)}), bf16[2048,256]{1,0:T(8,128)(2,1)}) %all-gather.11.cloned.1.call-update) | async-done | bytes 1048592 | tf_op jit(solution)/shard_map/all_gather | solution.py:115
  208.1 3.4 %multiply_convert_fusion = bf16[768,256]{1,0:T(8,128)(2,1)} fusion(bf16[768,256]{1,0:T(8,128)(2,1)} %copy-done.10, bf16[1,256]{1,0:T(2,128)(2,1)} %collective-permute-done.3, bf16[1,256]{1,0:T(2,128)(2,1)} %collective-permute-done.2, f32[256]{0:T(256)S(1)} %bitcast.90, f32[256]{0:T(256)S(1)} %bitcast.89, f32[256]{0:T(256)S(1)} %bitcast.88, ...), kind=kOutput, calls=%fused_computation.31 | convolution fusion | flops 808452096 | bytes 4984832 | tf_op jit(solution)/shard_map/dot_general | solution.py:119
  211.5 1.0 pad_maximum_fusion.6
  212.5 0.5 reshape.323
  213.0 0.3 copy.22
  213.3 0.5 reshape.324
  213.8 0.3 copy.23
  214.1 0.5 reshape.325
  214.6 0.3 copy.24
  214.9 0.1 pad_maximum_fusion
  215.0 0.5 fusion.1
  215.5 0.2 copy-done.9
  215.8 0.6 fusion
  216.4 0.9 fusion.7
  217.3 0.4 copy.29
  217.8 41.3 %all-gather.17.cloned.1.call-done = bf16[512,2048]{1,0:T(8,128)(2,1)} async-done(((bf16[512,256]{1,0:T(8,128)(2,1)}), bf16[512,2048]{1,0:T(8,128)(2,1)}) %all-gather.17.cloned.1.call-update) | async-done | bytes 2097168 | tf_op jit(solution)/shard_map/all_gather | solution.py:139
  259.1 5.0 %convolution_convert_fusion = bf16[768,2048]{1,0:T(8,128)(2,1)} fusion(bf16[512,2048]{1,0:T(8,128)(2,1)} %all-gather.17.cloned.1.call-done, bf16[768,256]{1,0:T(8,128)(2,1)S(1)} %copy-done.11, bf16[768,256]{1,0:T(8,128)(2,1)S(1)} %bitcast.87), kind=kOutput, calls=%fused_computation | convolution fusion | flops 1613758464 | bytes 6029312 | tf_op jit(solution)/shard_map/dot_general | solution.py:137
  264.1 36.1 %reduce-scatter.2.cloned.1.call-done = bf16[768,512]{1,0:T(8,128)(2,1)} async-done(((bf16[768,2048]{1,0:T(8,128)(2,1)}), bf16[768,512]{1,0:T(8,128)(2,1)}) %reduce-scatter.2.cloned.1.call-update) | async-done | bytes 786448 | tf_op jit(solution)/shard_map/reduce_scatter | solution.py:142
  300.2 1.4 convert_reduce_fusion
  301.6 5.9 %all-reduce = (f32[768]{0:T(1024)S(1)}, f32[768]{0:T(1024)S(1)}) all-reduce(f32[768]{0:T(1024)S(1)} %get-tuple-element.6, f32[768]{0:T(1024)S(1)} %get-tuple-element.5), channel_id=1, replica_groups=mesh['sp'=8,'tp'=4] {'tp'}, use_global_device_ids=true, to_apply=%region_6.7 | all-reduce | flops 1536 | bytes 12288 | tf_op jit(solution)/shard_map/psum | solution.py:146
  307.5 2.4 fusion.4
  (51 shorter events, 1.0 us)
Async XLA Ops:
  6.5 41.1 %copy-start.6 = (bf16[256,128]{1,0:T(8,128)(2,1)S(1)}, bf16[256,128]{1,0:T(8,128)(2,1)}, u32[]{:S(2)}) copy-start(bf16[256,128]{1,0:T(8,128)(2,1)} %param.15) | copy-start | bytes 196612
  6.5 75.0 %copy-start.7 = (bf16[3,256]{1,0:T(4,128)(2,1)S(1)}, bf16[3,256]{1,0:T(4,128)(2,1)}, u32[]{:S(2)}) copy-start(bf16[3,256]{1,0:T(4,128)(2,1)} %param.19) | copy-start | bytes 4612
  6.5 77.9 %all-gather.7.cloned.1.call-start = ((), (), s32[]{:S(2)}) async-start(), calls=%async_computation.1 | async-start | bytes 3932160 | tf_op jit(solution)/shard_map/all_gather | solution.py:104
  7.3 90.1 %all-gather.13.cloned.1.call-start = ((), (), s32[]{:S(2)}) async-start(), calls=%async_computation.4 | async-start | bytes 1179648 | tf_op jit(solution)/shard_map/all_gather | solution.py:116
  8.0 118.1 %all-gather.15.cloned.1.call-start = ((), (), s32[]{:S(2)}) async-start(), calls=%async_computation.5 | async-start | bytes 1179648 | tf_op jit(solution)/shard_map/all_gather | solution.py:114
  8.7 158.4 %all-gather.9.cloned.1.call-start = ((), (), s32[]{:S(2)}) async-start(), calls=%async_computation.2 | async-start | bytes 1179648 | tf_op jit(solution)/shard_map/all_gather | solution.py:111
  9.3 198.8 %all-gather.11.cloned.1.call-start = ((), (), s32[]{:S(2)}) async-start(), calls=%async_computation.3 | async-start | bytes 1179648 | tf_op jit(solution)/shard_map/all_gather | solution.py:115
  9.9 249.2 %all-gather.17.cloned.1.call-start = ((), (), s32[]{:S(2)}) async-start(), calls=%async_computation.6 | async-start | bytes 2359296 | tf_op jit(solution)/shard_map/all_gather | solution.py:139
  11.7 288.5 %reduce-scatter.2.cloned.1.call-start = ((), (), s32[]{:S(2)}) async-start(), calls=%async_computation.7 | async-start | bytes 3932160 | tf_op jit(solution)/shard_map/reduce_scatter | solution.py:142
  84.4 5.8 %copy-start = (bf16[768,2048]{1,0:T(8,128)(2,1)S(1)}, bf16[768,2048]{1,0:T(8,128)(2,1)}, u32[]{:S(2)}) copy-start(bf16[768,2048]{1,0:T(8,128)(2,1)} %all-gather.7.cloned.1.call-done) | copy-start | bytes 9437188
  87.7 2.5 copy-start.1
  92.1 119.4 %collective-permute-start = (bf16[128,256]{0,1:T(8,128)(2,1)}, bf16[128,256]{0,1:T(8,128)(2,1)}, u32[]{:S(2)}, u32[]{:S(2)}) collective-permute-start(bf16[128,256]{0,1:T(8,128)(2,1)} %get-tuple-element.16), channel_id=1, source_target_pairs={{0,4},{4,8},{8,12},{12,16},{16,20},{20,24},{24,28},{1,5},{5,9},{9,... | collective-permute-start | bytes 196616 | tf_op jit(solution)/shard_map/ppermute | solution.py:21
  96.1 115.5 %collective-permute-start.1 = (bf16[128,256]{0,1:T(8,128)(2,1)}, bf16[128,256]{0,1:T(8,128)(2,1)}, u32[]{:S(2)}, u32[]{:S(2)}) collective-permute-start(bf16[128,256]{0,1:T(8,128)(2,1)} %get-tuple-element.17), channel_id=1, source_target_pairs={{4,0},{8,4},{12,8},{16,12},{20,16},{24,20},{28,24},{5,1},{9,5},{13... | collective-permute-start | bytes 196616 | tf_op jit(solution)/shard_map/ppermute | solution.py:24
  128.5 3.6 %copy-start.10 = (bf16[768,256]{1,0:T(8,128)(2,1)}, bf16[768,256]{1,0:T(8,128)(2,1)S(1)}, u32[]{:S(2)}) copy-start(bf16[768,256]{1,0:T(8,128)(2,1)S(1)} %fusion.6) | copy-start | bytes 1179652
  129.1 79.0 %collective-permute-start.2 = (bf16[1,256]{1,0:T(2,128)(2,1)}, bf16[1,256]{1,0:T(2,128)(2,1)}, u32[]{:S(2)}, u32[]{:S(2)}) collective-permute-start(bf16[1,256]{1,0:T(2,128)(2,1)} %get-tuple-element.22), channel_id=1, source_target_pairs={{0,4},{4,8},{8,12},{12,16},{16,20},{20,24},{24,28},{1,5},{5,9},{9,... | collective-permute-start | bytes 1544 | tf_op jit(solution)/shard_map/ppermute | solution.py:21
  132.1 76.0 %collective-permute-start.3 = (bf16[1,256]{1,0:T(2,128)(2,1)S(1)}, bf16[1,256]{1,0:T(2,128)(2,1)}, u32[]{:S(2)}, u32[]{:S(2)}) collective-permute-start(bf16[1,256]{1,0:T(2,128)(2,1)S(1)} %get-tuple-element.23), channel_id=1, source_target_pairs={{4,0},{8,4},{12,8},{16,12},{20,16},{24,20},{28,24},{5,1},{9,5},{13... | collective-permute-start | bytes 1544 | tf_op jit(solution)/shard_map/ppermute | solution.py:24
  167.1 2.4 copy-start.3
  169.4 1.0 copy-start.2
  213.8 1.3 copy-start.4
  213.8 1.3 copy-start.5
  215.0 0.7 copy-start.9
  216.4 42.7 %copy-start.11 = (bf16[768,256]{1,0:T(8,128)(2,1)S(1)}, bf16[768,256]{1,0:T(8,128)(2,1)}, u32[]{:S(2)}) copy-start(bf16[768,256]{1,0:T(8,128)(2,1)} %multiply_convert_fusion) | copy-start | bytes 1179652
  264.1 43.4 %copy-start.8 = (f32[512]{0:T(512)S(1)}, f32[512]{0:T(512)}, u32[]{:S(2)}) copy-start(f32[512]{0:T(512)} %param.23) | copy-start | bytes 6148
Sparse Core Ops, SparseCore 0:
  8.9 31.2 all-gather.6
  42.3 41.5 all-gather.12
  86.0 40.0 all-gather.14
  128.1 38.9 all-gather.8
  169.1 38.9 all-gather.10
  210.0 49.0 all-gather.16
  264.3 35.8 reduce-scatter.1
where the time goes:
time: 317 us
  waiting for transfers between devices  174 us (55%)
  blocking collectives  75.4 us (24%)
  matrix products  22.1 us (7%)
  other arithmetic  14.6 us (5%)
  between operations  13.8 us (4%)
  starting transfers between devices  9.93 us (3%)
  local copies, waits for them, and re-layouts  6.65 us (2%)
    all_gather x1, waiting for transfers between devices, body(): lax.all_gather(stacked, 'sp', axis=1, tiled=True)  41.3 us
    reduce_scatter x1, waiting for transfers between devices, body(): lax.psum_scatter(partial_sums.astype(jnp.bfloat16), 'tp', scatter_dimensi...  36.1 us
    all_gather x1, blocking collectives, body(): lax.all_gather(key_projection, 'sp', axis=0, tiled=True)  35.7 us
    all_gather x1, waiting for transfers between devices, body(): lax.all_gather(conv_gate_out, 'sp', axis=0, tiled=True)  34.5 us
    all_gather x1, blocking collectives, body(): lax.all_gather(value_projection, 'sp', axis=0, tiled=True)  33.9 us
    all_gather x1, waiting for transfers between devices, body(): lax.all_gather(query_weight, 'sp', axis=0, tiled=True)  33.5 us
    all_gather x1, waiting for transfers between devices, body(): lax.all_gather(conv_in_weight, 'sp', axis=0, tiled=True)  25.6 us
    dot_general x6, matrix products, body(): jnp.dot(whole, piece, preferred_element_type=jnp.float32)  15.7 us
  transfers between devices with their start and end apart: 11, of which 5 were waited for; matrix products, arithmetic and copies ran while one was open for 11% of the time, Pallas kernels for 0%

commit v1 on v0

--- a/solution.py
+++ b/solution.py
@@ -1,6 +1,10 @@
+import functools
+
 import jax
 import jax.numpy as jnp
 from jax import lax
+from jax.experimental import pallas as pl
+from jax.experimental.pallas import tpu as pltpu
 from jax.sharding import PartitionSpec as P
 
 HEAD_SIZE = 128
@@ -87,7 +91,7 @@
     return (gate_after * conv_mix).astype(jnp.bfloat16)
 
 
-def body(
+def plain_body(
     tokens,
     query_weight,
     key_projection,
@@ -150,9 +154,423 @@
     return normed.astype(jnp.bfloat16)
 
 
+def fused_kernel(
+    outer, tp, tokens_ref, wq_ref, wk_ref, wv_ref, wi_ref, wgo_ref, wgi_ref, wa_ref, wc_ref,
+    taps_ref, sink_ref, gain_ref, cosr_ref, sinr_ref, cosc_ref, sinc_ref, out_ref,
+    tok, a_buf, b_buf, c_buf, q_buf, kv, proj, sec, mix, stage, rbuf, loc, my_stat, stats,
+    local_sem, w_send, w_recv, t_send, t_recv, halo_send, halo_recv, rs_send, rs_recv,
+    st_send, st_recv,
+):
+    f32, bf16 = jnp.float32, jnp.bfloat16
+    s, t = lax.axis_index("sp"), lax.axis_index("tp")
+    span = 2 * outer
+    o, i = lax.div(s, 2), lax.rem(s, 2)
+    odd = lax.rem(o, 2)
+    mate = o + 1 - 2 * odd
+    partner = 2 * o + 1 - i
+    items = tokens_ref.shape[0]
+    blocks = items // WINDOW
+    edge = 16
+    sends = []
+    always = s >= 0
+
+    def remote(src, dst, send_sem, recv_sem, dev):
+        return pltpu.make_async_remote_copy(
+            src_ref=src, dst_ref=dst, send_sem=send_sem, recv_sem=recv_sem,
+            device_id=dev, device_id_type=pl.DeviceIdType.MESH,
+        )
+
+    def post(cond, *args):
+        def run():
+            remote(*args).start()
+
+        pl.when(cond)(run)
+        sends.append((cond, args))
+
+    half_c = wa_ref.shape[0]
+    qw, kw = wq_ref.shape[1], wk_ref.shape[1]
+    cw = wi_ref.shape[1]
+    own = [
+        (tokens_ref, tok.at[t]),
+        (wq_ref, a_buf.at[s, :, pl.ds(0, qw)]),
+        (wk_ref, a_buf.at[s, :, pl.ds(qw, kw)]),
+        (wv_ref, a_buf.at[s, :, pl.ds(qw + kw, kw)]),
+        (wi_ref, b_buf.at[s, :, pl.ds(0, cw)]),
+        (wgo_ref, b_buf.at[s, :, pl.ds(cw, cw)]),
+        (wgi_ref, b_buf.at[s, :, pl.ds(2 * cw, cw)]),
+        (wa_ref, c_buf.at[s, pl.ds(0, half_c)]),
+        (wc_ref, c_buf.at[s, pl.ds(half_c, half_c)]),
+    ]
+    local = [
+        pltpu.make_async_copy(a, b, local_sem.at[n]) for n, (a, b) in enumerate(own)
+    ]
+    for copy in local:
+        copy.start()
+
+    barrier = pltpu.get_barrier_semaphore()
+    greet = [(s + 1 < span, (s + 1, t)), (s > 0, (s - 1, t)),
+             (o + 1 < outer, (s + 2, t)), (o > 0, (s - 2, t))]
+    greet += [(always, (s, lax.rem(t + d, tp))) for d in range(1, tp)]
+    for cond, dev in greet:
+        @pl.when(cond)
+        def _(dev=dev):
+            pl.semaphore_signal(barrier, inc=1, device_id=dev, device_id_type=pl.DeviceIdType.MESH)
+    pl.semaphore_wait(barrier, sum(cond.astype(jnp.int32) for cond, dev in greet))
+
+    bufs = (a_buf, b_buf, c_buf)
+
+    def unit(p, piece, h):
+        rows = bufs[p].shape[1] // 2
+        return bufs[p].at[piece, pl.ds(h * rows, rows)]
+
+    def send(p, piece, h, d, dev, cond):
+        ref = unit(p, piece, h)
+        post(cond, ref, ref, w_send.at[p, d, piece, h], w_recv.at[p, piece, h], (dev, t))
+
+    def recv(p, piece, h):
+        ref = unit(p, piece, h)
+        remote(ref, ref, w_send.at[p, 0, piece, h], w_recv.at[p, piece, h], (partner, t)).wait_recv()
+
+    def step0(p):
+        for h in range(2):
+            send(p, s, h, 0, s + 2, o + 1 < outer)
+            send(p, s, h, 1, s - 2, o > 0)
+            send(p, s, h, 2, partner, always)
+
+    def step0_partner(p):
+        recv(p, partner, 0)
+        recv(p, partner, 1)
+        send(p, partner, 1, 3, 2 * mate + i, always)
+
+    def step(p, k):
+        for h in range(2):
+            low, high = s - 2 * k, s + 2 * k
+            has_low, has_high = o >= k, o + k < outer
+            pl.when(has_low)(lambda: recv(p, low, h))
+            send(p, low, h, 0, s + 2, has_low & (o + 1 < outer))
+            skip = h == 1 and k == 1
+            send(p, low, h, 2, partner, (has_low & (odd == 0)) if skip else has_low)
+            pl.when(has_high)(lambda: recv(p, high, h))
+            send(p, high, h, 1, s - 2, has_high & (o > 0))
+            send(p, high, h, 2, partner, (has_high & (odd == 1)) if skip else has_high)
+
+    def take(p, k, low):
+        base = partner - 2 * k if low else partner + 2 * k
+        for h in range(2):
+            recv(p, base, h)
+
+    def take_all(p):
+        for k in range(1, outer):
+            pl.when(o >= k)(lambda: take(p, k, True))
+            pl.when(o + k < outer)(lambda: take(p, k, False))
+
+    for copy in local[:4]:
+        copy.wait()
+    sibling = t + 1 - 2 * lax.rem(t, 2)
+    post(always, tok.at[t], tok.at[t], t_send.at[0], t_recv.at[t], (s, sibling))
+    across = [lax.rem(t + 2 * d, tp) for d in range(1, tp // 2)]
+    for n, far in enumerate(across):
+        post(always, tok.at[t], tok.at[t], t_send.at[1 + n], t_recv.at[t], (s, far))
+
+    def wait_tok(src):
+        remote(tok.at[src], tok.at[src], t_send.at[0], t_recv.at[src], (s, sibling)).wait_recv()
+
+    step0(0)
+    for copy in local[4:]:
+        copy.wait()
+    step0_partner(0)
+    step(0, 1)
+    step0(1)
+    for k in range(2, outer):
+        step(0, k)
+    for n, far in enumerate(across):
+        wait_tok(far)
+        post(always, tok.at[far], tok.at[far], t_send.at[tp // 2 + n], t_recv.at[far], (s, sibling))
+    wait_tok(sibling)
+    for far in across:
+        wait_tok(far + 1 - 2 * lax.rem(far, 2))
+    take_all(0)
+
+    tile = 256
+    depth = a_buf.shape[1]
+    per = tok.shape[2] // depth
+
+    def project(buf, rows, cols):
+        total = None
+        for piece in range(span):
+            lane = (piece % per) * depth
+            term = jnp.dot(
+                tok[piece // per, rows, lane : lane + depth], buf[piece, :, cols],
+                preferred_element_type=f32,
+            )
+            total = term if total is None else total + term
+        return total
+
+    lane_row = lax.broadcasted_iota(jnp.int32, (1, HEAD_SIZE), 1)
+    first_half = lax.rem(lane_row, HEAD_SIZE // 2) < HEAD_SIZE // 4
+    left_lanes = (lane_row < HEAD_SIZE // 2)[None]
+    for n in range(items // tile):
+        rows = pl.ds(n * tile, tile)
+        grid_rows = tile // GRID
+
+        def table(row_ref, col_ref):
+            r = row_ref[pl.ds(n * grid_rows, grid_rows), :][:, None, :]
+            c = col_ref[...][None]
+            r = jnp.broadcast_to(r, (grid_rows, GRID, HEAD_SIZE))
+            c = jnp.broadcast_to(c, (grid_rows, GRID, HEAD_SIZE))
+            return jnp.where(left_lanes, r, c).reshape(tile, HEAD_SIZE)
+
+        cosine = table(cosr_ref, cosc_ref)
+        sine = table(sinr_ref, sinc_ref)
+        sine = jnp.where(first_half, -sine, sine)
+        raw = project(a_buf, rows, slice(None))
+
+        def turn(u):
+            other = jnp.where(
+                first_half, pltpu.roll(u, HEAD_SIZE - HEAD_SIZE // 4, 1), pltpu.roll(u, HEAD_SIZE // 4, 1)
+            )
+            return (u * cosine + other * sine).astype(bf16)
+
+        for g in range(qw // HEAD_SIZE):
+            cols = slice(g * HEAD_SIZE, (g + 1) * HEAD_SIZE)
+            q_buf[rows, cols] = turn(raw[:, cols])
+        inner = pl.ds(WINDOW + n * tile, tile)
+        kv[inner, :kw] = turn(raw[:, qw : qw + kw])
+        kv[inner, kw:] = raw[:, qw + kw :].astype(bf16)
+
+    has_left, has_right = s > 0, s + 1 < span
+
+    def halo(ref, width, base):
+        last = ref.shape[0] - width
+        post(has_right, ref.at[pl.ds(last - width, width)], ref.at[pl.ds(0, width)],
+             halo_send.at[base], halo_recv.at[base], (s + 1, t))
+        post(has_left, ref.at[pl.ds(width, width)], ref.at[pl.ds(last, width)],
+             halo_send.at[base + 1], halo_recv.at[base + 1], (s - 1, t))
+
+    def halo_wait(ref, width, base):
+        last = ref.shape[0] - width
+        for n, (cond, start) in enumerate(((has_left, 0), (has_right, last))):
+            dst = ref.at[pl.ds(start, width)]
+
+            @pl.when(cond)
+            def _():
+                remote(dst, dst, halo_send.at[base + n], halo_recv.at[base + n], (partner, t)).wait_recv()
+
+            @pl.when(jnp.logical_not(cond))
+            def _():
+                ref[pl.ds(start, width), :] = jnp.zeros((width, ref.shape[1]), ref.dtype)
+
+    halo(kv, WINDOW, 0)
+
+    group = qw // HEAD_SIZE
+    shape = (group * WINDOW, 3 * WINDOW)
+
+    def attend_block(b):
+        rows = pl.ds(b * WINDOW, WINDOW)
+        band = pl.ds(b * WINDOW, 3 * WINDOW)
+        q = jnp.concatenate(
+            [q_buf[rows, g * HEAD_SIZE : (g + 1) * HEAD_SIZE] for g in range(group)], 0
+        )
+        scores = lax.dot_general(
+            q, kv[band, :kw], (((1,), (1,)), ((), ())), preferred_element_type=f32
+        ) * HEAD_SIZE ** (-0.5)
+        row = lax.broadcasted_iota(jnp.int32, shape, 0)
+        col = lax.broadcasted_iota(jnp.int32, shape, 1)
+        gap = col - WINDOW - lax.rem(row, WINDOW)
+        position = s * items + (b - 1) * WINDOW + col
+        valid = (jnp.abs(gap) <= WINDOW) & (position >= 0) & (position < items * span)
+        scores = jnp.where(valid, scores, NEG_BIG)
+        head = lax.broadcasted_iota(jnp.int32, (group * WINDOW, 1), 0) // WINDOW
+        sink = jnp.zeros((group * WINDOW, 1), f32)
+        for g in range(group):
+            sink = jnp.where(head == g, sink_ref[g], sink)
+        top = jnp.maximum(jnp.max(scores, -1, keepdims=True), sink)
+        weights = jnp.exp(scores - top)
+        denominator = jnp.sum(weights, -1, keepdims=True) + jnp.exp(sink - top)
+        probs = (weights / denominator).astype(bf16)
+        mixed = jnp.dot(probs, kv[band, kw:], preferred_element_type=f32).astype(bf16)
+        for g in range(group):
+            mix[rows, g * HEAD_SIZE : (g + 1) * HEAD_SIZE] = mixed[g * WINDOW : (g + 1) * WINDOW]
+
+    step0_partner(1)
+    step(1, 1)
+    for b in range(1, blocks - 1):
+        attend_block(b)
+    step(1, 2) if outer > 2 else None
+    step0(2)
+    halo_wait(kv, WINDOW, 0)
+    attend_block(0)
+    attend_block(blocks - 1)
+    for k in range(3, outer):
+        step(1, k)
+    take_all(1)
+
+    for n in range(items // tile):
+        rows = pl.ds(n * tile, tile)
+        inner = pl.ds(edge + n * tile, tile)
+        conv_input = project(b_buf, rows, slice(0, cw))
+        before = project(b_buf, rows, slice(2 * cw, 3 * cw))
+        sec[inner, :] = (before * conv_input).astype(bf16)
+    halo(sec, edge, 2)
+    for n in range(items // tile):
+        rows = pl.ds(n * tile, tile)
+        proj[rows, :] = project(b_buf, rows, slice(cw, 2 * cw))
+    step0_partner(2)
+    step(2, 1)
+    halo_wait(sec, edge, 2)
+    full = sec[...].astype(f32)
+    taps = taps_ref[...].astype(f32)
+    length = full.shape[0]
+    conv = (
+        pltpu.roll(full, 1, 0) * taps[0:1]
+        + full * taps[1:2]
+        + pltpu.roll(full, length - 1, 0) * taps[2:3]
+    )
+    mix[:, qw:] = (proj[...] * conv[edge : edge + items]).astype(bf16)
+
+    width = c_buf.shape[2]
+
+    def produce(owner):
+        def one(n, carry):
+            rows = pl.ds(pl.multiple_of(n * tile, tile), tile)
+            x = mix[rows, :]
+            for j in range(2):
+                y = jnp.dot(x, c_buf[2 * owner + j], preferred_element_type=f32)
+                stage[owner, rows, j * width : (j + 1) * width] = y.astype(bf16)
+
+                @pl.when(owner == t)
+                def _():
+                    loc[rows, j * width : (j + 1) * width] = y
+            return carry
+
+        lax.fori_loop(0, items // tile, one, 0)
+
+    def give(cond, owner):
+        pl.when(cond)(lambda: produce(owner))
+        post(cond & (owner != t), stage.at[owner], rbuf.at[t], rs_send.at[owner], rs_recv.at[t], (s, owner))
+
+    give(always, o)
+    for k in range(1, outer):
+        if k > 1:
+            step(2, k)
+        pl.when(o >= k)(lambda: take(2, k, True))
+        pl.when(o + k < outer)(lambda: take(2, k, False))
+        give(o >= k, o - k)
+        give(o + k < outer, o + k)
+
+    summed = loc[...]
+    for d in range(1, tp):
+        src = lax.rem(t + d, tp)
+        remote(rbuf.at[src], rbuf.at[src], rs_send.at[0], rs_recv.at[src], (s, src)).wait_recv()
+        summed = summed + rbuf[src].astype(f32)
+    loc[...] = summed
+    lane = lax.broadcasted_iota(jnp.int32, (items, 128), 1)
+    both = jnp.where(
+        lane == 0, jnp.sum(summed, 1, keepdims=True), jnp.sum(summed * summed, 1, keepdims=True)
+    )
+    my_stat[...] = jnp.transpose(both)[:8]
+    for d in range(1, tp):
+        dst = lax.rem(t + d, tp)
+        post(always, my_stat, stats.at[t], st_send.at[d], st_recv.at[t], (s, dst))
+    total = my_stat[...]
+    for d in range(1, tp):
+        src = lax.rem(t + d, tp)
+        remote(stats.at[src], stats.at[src], st_send.at[0], st_recv.at[src], (s, src)).wait_recv()
+        total = total + stats[src]
+    total = total * (1.0 / (tp * out_ref.shape[1]))
+    total = jnp.transpose(jnp.concatenate([total] * 16, 0))
+    mean = total[:, 0:1]
+    spread = total[:, 1:2] - mean * mean
+    out_ref[...] = ((loc[...] - mean) * lax.rsqrt(spread + EPS) * gain_ref[...]).astype(bf16)
+
+    for cond, args in sends:
+        pl.when(cond)(lambda args=args: remote(*args).wait_send())
+
+
+def small_tables(offset, items):
+    half = HEAD_SIZE // 2
+    inverse = THETA ** (-jnp.arange(0, half, 2, dtype=jnp.float32) / half)
+    inverse = jnp.concatenate([inverse] * 4)[None]
+    row = (offset // GRID + jnp.arange(items // GRID, dtype=jnp.int32)).astype(jnp.float32)
+    column = jnp.arange(GRID, dtype=jnp.int32).astype(jnp.float32)
+    row, column = row[:, None] * inverse, column[:, None] * inverse
+    return jnp.cos(row), jnp.sin(row), jnp.cos(column), jnp.sin(column)
+
+
+def body(
+    sizes, tokens, query_weight, key_projection, value_projection, conv_in_weight, conv_gate_out,
+    conv_gate_in, conv_taps, head_sink_logit, out_attn_weight, out_conv_weight, out_gain,
+):
+    span, tp = sizes["sp"], sizes["tp"]
+    items, features = tokens.shape
+    depth = query_weight.shape[0]
+    group = query_weight.shape[1] // HEAD_SIZE
+    fits = (
+        span == 2 * tp and tp % 2 == 0 and depth % 128 == 0 and features == 2 * depth
+        and out_attn_weight.shape[1] % 128 == 0 and items % (2 * WINDOW) == 0
+        and key_projection.shape[1] == HEAD_SIZE and conv_in_weight.shape[1] % 128 == 0
+        and out_attn_weight.shape[0] == out_conv_weight.shape[0]
+    )
+    if not fits:
+        return plain_body(
+            tokens, query_weight, key_projection, value_projection, conv_in_weight, conv_gate_out,
+            conv_gate_in, conv_taps, head_sink_logit, out_attn_weight, out_conv_weight, out_gain,
+        )
+    tables = small_tables(lax.axis_index("sp") * items, items)
+    outer = span // 2
+    f32, bf16 = jnp.float32, jnp.bfloat16
+    qw, kw, cw = query_weight.shape[1], key_projection.shape[1], conv_in_weight.shape[1]
+    mixer = out_attn_weight.shape[0] + out_conv_weight.shape[0]
+    own_width = out_gain.shape[0]
+    dma = pltpu.SemaphoreType.DMA
+    anywhere = pl.BlockSpec(memory_space=pl.ANY)
+    vmem = pl.BlockSpec(memory_space=pltpu.VMEM)
+    smem = pl.BlockSpec(memory_space=pltpu.SMEM)
+    return pl.pallas_call(
+        functools.partial(fused_kernel, outer, tp),
+        out_shape=jax.ShapeDtypeStruct((items, own_width), bf16),
+        in_specs=[anywhere] * 9 + [vmem, smem, vmem] + [vmem] * 4,
+        out_specs=vmem,
+        scratch_shapes=[
+            pltpu.VMEM((tp, items, features), bf16),
+            pltpu.VMEM((span, depth, qw + 2 * kw), bf16),
+            pltpu.VMEM((span, depth, 3 * cw), bf16),
+            pltpu.VMEM((span, mixer, out_attn_weight.shape[1]), bf16),
+            pltpu.VMEM((items, qw), bf16),
+            pltpu.VMEM((items + 2 * WINDOW, 2 * kw), bf16),
+            pltpu.VMEM((items, cw), f32),
+            pltpu.VMEM((items + 32, cw), bf16),
+            pltpu.VMEM((items, mixer), bf16),
+            pltpu.VMEM((tp, items, own_width), bf16),
+            pltpu.VMEM((tp, items, own_width), bf16),
+            pltpu.VMEM((items, own_width), f32),
+            pltpu.VMEM((8, items), f32),
+            pltpu.VMEM((tp, 8, items), f32),
+            dma((9,)),
+            dma((3, 4, span, 2)),
+            dma((3, span, 2)),
+            dma((tp,)),
+            dma((tp,)),
+            dma((4,)),
+            dma((4,)),
+            dma((tp,)),
+            dma((tp,)),
+            dma((tp,)),
+            dma((tp,)),
+        ],
+        compiler_params=pltpu.CompilerParams(
+            collective_id=0, has_side_effects=True, vmem_limit_bytes=60 * 2**20
+        ),
+    )(
+        tokens, query_weight, key_projection, value_projection, conv_in_weight, conv_gate_out,
+        conv_gate_in, out_attn_weight, out_conv_weight, conv_taps, head_sink_logit,
+        out_gain[None], *tables,
+    )
+
+
 def solution(mesh):
     return jax.shard_map(
-        body,
+        functools.partial(body, dict(mesh.shape)),
         mesh=mesh,
         in_specs=(
             P("sp", "tp"),

time: 317 us -> 132 us (0.42)
  waiting for transfers between devices: 174 us -> 0 us
  Pallas kernels: 0 us -> 128 us
  blocking collectives: 75.4 us -> 0 us
  matrix products: 22.1 us -> 0 us
  between operations: 13.8 us -> 0.01 us
  other arithmetic: 14.6 us -> 1.63 us
  starting transfers between devices: 9.93 us -> 0 us
  local copies, waits for them, and re-layouts: 6.65 us -> 2.06 us
    all_gather x6 -> x0, waiting for transfers between devices: 135 us -> none  [the longest x1 41.3 us: body(): lax.all_gather(stacked, 'sp', axis=1, tiled=True)]
    pallas_call x0 -> x1, Pallas kernels: none -> 128 us  [body(): pl.pallas_call(functools.partial(fused_kernel, outer, tp), out_shape=jax....]
    all_gather x2 -> x0, blocking collectives: 69.6 us -> none  [the longest x1 35.7 us: body(): lax.all_gather(key_projection, 'sp', axis=0, tiled=True)]
    reduce_scatter x1 -> x0, waiting for transfers between devices: 36.1 us -> none  [body(): lax.psum_scatter(partial_sums.astype(jnp.bfloat16), 'tp', scatter_dimensi...]
    dot_general x9 -> x0, matrix products: 22.1 us -> none  [the longest x6 15.7 us: body(): jnp.dot(whole, piece, preferred_element_type=jnp.float32)]
    ppermute x4 -> x0, starting transfers between devices: 9.7 us -> none  [the longest x2 6.96 us: with_halo(): lax.ppermute(lax.slice_in_dim(block, block.shape[dim] - width, None, axis...]
    psum x1 -> x0, blocking collectives: 5.86 us -> none  [body(): lax.psum((jnp.sum(summed, 1), jnp.sum(summed * summed, 1)), 'tp')]
    concatenate x5 -> x1, other arithmetic: 3.43 us -> 0.08 us  [small_tables(): inverse = jnp.concatenate([inverse] * 4)[None]]
  transfers between devices with their start and end apart: 11 -> 0, of which waited for: 5 -> 0; matrix products, arithmetic and copies ran while one was open for 11% -> 0% of each run, Pallas kernels for 0% -> 0%
where the time goes in v1:
time: 132 us
  Pallas kernels  128 us (97%)
  local copies, waits for them, and re-layouts  2.06 us (2%)
  other arithmetic  1.63 us (1%)
    pallas_call x1, Pallas kernels, body(): pl.pallas_call(functools.partial(fused_kernel, outer, tp), out_shape=jax....  128 us

profile of v1, /device:TPU:0, one launch (start us, length us, event | category | flops | bytes accessed | tf_op | source)
XLA Modules:
  0.0 131.9 jit_solution(14880493517748207118)
XLA Ops:
  0.0 0.1 pad_maximum_fusion
  0.1 0.7 multiply_sine_fusion.1
  0.8 0.8 multiply_sine_fusion
  1.6 128.2 %shard_map.118 = bf16[768,512]{1,0:T(8,128)(2,1)} custom-call(bf16[768,512]{1,0:T(8,128)(2,1)} %tokens_ref.1, bf16[256,256]{1,0:T(8,128)(2,1)} %wq_ref.1, bf16[256,128]{1,0:T(8,128)(2,1)} %wk_ref.1, bf16[256,128]{1,0:T(8,128)(2,1)} %wv_ref.1, bf16[256,256]{1,0:T(8,128)(2,1)} %wi_ref.1, bf16[256,256]{1,0:T(8,128)(2,1)} %wgo_ref.1, bf16[256,256]{1,0:T(8,128)(2,1)} %wgi_ref.1, ...), custom_call_target="tpu_custom_call" | custom-call | tf_op jit(solution)/shard_map/pallas_call | solution.py:529
  129.8 2.1 %copy.14 = bf16[768,512]{1,0:T(8,128)(2,1)} copy(bf16[768,512]{1,0:T(8,128)(2,1)} %shard_map.118) | data formatting | bytes 1572864
  (3 shorter events, 0.0 us)

commit v2 on v1

--- a/solution.py
+++ b/solution.py
@@ -157,8 +157,8 @@
 def fused_kernel(
     outer, tp, tokens_ref, wq_ref, wk_ref, wv_ref, wi_ref, wgo_ref, wgi_ref, wa_ref, wc_ref,
     taps_ref, sink_ref, gain_ref, cosr_ref, sinr_ref, cosc_ref, sinc_ref, out_ref,
-    tok, a_buf, b_buf, c_buf, q_buf, kv, proj, sec, mix, stage, rbuf, loc, my_stat, stats,
-    local_sem, w_send, w_recv, t_send, t_recv, halo_send, halo_recv, rs_send, rs_recv,
+    tok, a_buf, b_buf, c_buf, q_buf, kv, proj, sec, mix, stage, rbuf, pair, pre, loc, my_stat, stats,
+    local_sem, w_send, w_recv, t_send, t_recv, halo_send, halo_recv, rs_send, rs_recv, pair_recv,
     st_send, st_recv,
 ):
     f32, bf16 = jnp.float32, jnp.bfloat16
@@ -405,18 +405,21 @@
         step(1, k)
     take_all(1)
 
+    step0_partner(2)
     for n in range(items // tile):
         rows = pl.ds(n * tile, tile)
         inner = pl.ds(edge + n * tile, tile)
         conv_input = project(b_buf, rows, slice(0, cw))
         before = project(b_buf, rows, slice(2 * cw, 3 * cw))
         sec[inner, :] = (before * conv_input).astype(bf16)
+        if n == 0:
+            step(2, 1)
     halo(sec, edge, 2)
+    if outer > 2:
+        step(2, 2)
     for n in range(items // tile):
         rows = pl.ds(n * tile, tile)
         proj[rows, :] = project(b_buf, rows, slice(cw, 2 * cw))
-    step0_partner(2)
-    step(2, 1)
     halo_wait(sec, edge, 2)
     full = sec[...].astype(f32)
     taps = taps_ref[...].astype(f32)
@@ -430,39 +433,71 @@
 
     width = c_buf.shape[2]
 
-    def produce(owner):
+    core = lax.rem(t, 2)
+
+    def produce(owner, slot):
+        mine = lax.rem(owner, 2) == core
+
         def one(n, carry):
             rows = pl.ds(pl.multiple_of(n * tile, tile), tile)
             x = mix[rows, :]
             for j in range(2):
+                cols = slice(j * width, (j + 1) * width)
                 y = jnp.dot(x, c_buf[2 * owner + j], preferred_element_type=f32)
-                stage[owner, rows, j * width : (j + 1) * width] = y.astype(bf16)
 
                 @pl.when(owner == t)
                 def _():
-                    loc[rows, j * width : (j + 1) * width] = y
+                    loc[rows, cols] = y
+
+                @pl.when(mine & (owner != t))
+                def _():
+                    pre[slot, rows, cols] = y
+
+                @pl.when(jnp.logical_not(mine))
+                def _():
+                    stage[owner, rows, cols] = y.astype(bf16)
             return carry
 
         lax.fori_loop(0, items // tile, one, 0)
 
-    def give(cond, owner):
-        pl.when(cond)(lambda: produce(owner))
-        post(cond & (owner != t), stage.at[owner], rbuf.at[t], rs_send.at[owner], rs_recv.at[t], (s, owner))
-
-    give(always, o)
+    def pair_wait(owner):
+        ref = pair.at[lax.div(owner, 2)]
+        remote(ref, ref, rs_send.at[0], pair_recv.at[lax.div(owner, 2)], (s, sibling)).wait_recv()
+
+    def give(cond, owner, slot):
+        pl.when(cond)(lambda: produce(owner, slot))
+        post(cond & (lax.rem(owner, 2) != core), stage.at[owner], pair.at[lax.div(owner, 2)],
+             rs_send.at[owner], pair_recv.at[lax.div(owner, 2)], (s, sibling))
+
+    def finish(cond, owner, slot):
+        active = cond & (lax.rem(owner, 2) == core) & (owner != t)
+
+        @pl.when(active)
+        def _():
+            pair_wait(owner)
+            stage[owner] = (pre[slot] + pair[lax.div(owner, 2)].astype(f32)).astype(bf16)
+
+        post(active, stage.at[owner], rbuf.at[lax.div(t, 2)], rs_send.at[owner],
+             rs_recv.at[lax.div(t, 2)], (s, owner))
+
+    give(always, o, 0)
+    finish(always, o, 0)
     for k in range(1, outer):
-        if k > 1:
+        if k > 2:
             step(2, k)
         pl.when(o >= k)(lambda: take(2, k, True))
+        give(o >= k, o - k, 0)
         pl.when(o + k < outer)(lambda: take(2, k, False))
-        give(o >= k, o - k)
-        give(o + k < outer, o + k)
-
-    summed = loc[...]
-    for d in range(1, tp):
-        src = lax.rem(t + d, tp)
-        remote(rbuf.at[src], rbuf.at[src], rs_send.at[0], rs_recv.at[src], (s, src)).wait_recv()
-        summed = summed + rbuf[src].astype(f32)
+        give(o + k < outer, o + k, 1)
+        finish(o >= k, o - k, 0)
+        finish(o + k < outer, o + k, 1)
+
+    pair_wait(t)
+    summed = loc[...] + pair[lax.div(t, 2)].astype(f32)
+    for far in across:
+        slot = lax.div(far, 2)
+        remote(rbuf.at[slot], rbuf.at[slot], rs_send.at[0], rs_recv.at[slot], (s, far)).wait_recv()
+        summed = summed + rbuf[slot].astype(f32)
     loc[...] = summed
     lane = lax.broadcasted_iota(jnp.int32, (items, 128), 1)
     both = jnp.where(
@@ -542,7 +577,9 @@
             pltpu.VMEM((items + 32, cw), bf16),
             pltpu.VMEM((items, mixer), bf16),
             pltpu.VMEM((tp, items, own_width), bf16),
-            pltpu.VMEM((tp, items, own_width), bf16),
+            pltpu.VMEM((tp // 2, items, own_width), bf16),
+            pltpu.VMEM((tp // 2, items, own_width), bf16),
+            pltpu.VMEM((2, items, own_width), f32),
             pltpu.VMEM((items, own_width), f32),
             pltpu.VMEM((8, items), f32),
             pltpu.VMEM((tp, 8, items), f32),
@@ -555,6 +592,7 @@
             dma((4,)),
             dma((tp,)),
             dma((tp,)),
+            dma((tp // 2,)),
             dma((tp,)),
             dma((tp,)),
         ],

time: 132 us -> 117 us (0.89)
  Pallas kernels: 128 us -> 113 us
    pallas_call x1, Pallas kernels: 128 us -> 113 us  [body(): pl.pallas_call(functools.partial(fused_kernel, outer, tp), out_shape=jax....]
where the time goes in v2:
time: 117 us
  Pallas kernels  113 us (97%)
  local copies, waits for them, and re-layouts  2.06 us (2%)
  other arithmetic  1.63 us (1%)
    pallas_call x1, Pallas kernels, body(): pl.pallas_call(functools.partial(fused_kernel, outer, tp), out_shape=jax....  113 us

profile of v2, /device:TPU:0, one launch (start us, length us, event | category | flops | bytes accessed | tf_op | source)
XLA Modules:
  0.0 117.0 jit_solution(12023602561109697351)
XLA Ops:
  0.0 0.1 pad_maximum_fusion
  0.1 0.7 multiply_sine_fusion.1
  0.8 0.8 multiply_sine_fusion
  1.6 113.3 %shard_map.118 = bf16[768,512]{1,0:T(8,128)(2,1)} custom-call(bf16[768,512]{1,0:T(8,128)(2,1)} %tokens_ref.1, bf16[256,256]{1,0:T(8,128)(2,1)} %wq_ref.1, bf16[256,128]{1,0:T(8,128)(2,1)} %wk_ref.1, bf16[256,128]{1,0:T(8,128)(2,1)} %wv_ref.1, bf16[256,256]{1,0:T(8,128)(2,1)} %wi_ref.1, bf16[256,256]{1,0:T(8,128)(2,1)} %wgo_ref.1, bf16[256,256]{1,0:T(8,128)(2,1)} %wgi_ref.1, ...), custom_call_target="tpu_custom_call" | custom-call | tf_op jit(solution)/shard_map/pallas_call | solution.py:564
  115.0 2.1 %copy.14 = bf16[768,512]{1,0:T(8,128)(2,1)} copy(bf16[768,512]{1,0:T(8,128)(2,1)} %shard_map.118) | data formatting | bytes 1572864
  (3 shorter events, 0.0 us)

commit v3 on v2

--- a/solution.py
+++ b/solution.py
@@ -392,8 +392,32 @@
         for g in range(group):
             mix[rows, g * HEAD_SIZE : (g + 1) * HEAD_SIZE] = mixed[g * WINDOW : (g + 1) * WINDOW]
 
+    def add(piece, first=False):
+        source, lane = lax.div(piece, per), lax.rem(piece, per) * depth
+
+        def one(n, carry):
+            rows = pl.ds(pl.multiple_of(n * tile, tile), tile)
+            x = tok[source, rows, pl.ds(pl.multiple_of(lane, depth), depth)]
+            term = jnp.dot(x, b_buf[piece], preferred_element_type=f32)
+            proj[rows, :] = term if first else proj[rows, :] + term
+            return carry
+
+        lax.fori_loop(0, items // tile, one, 0)
+
+    def add_pair(k, base):
+        pl.when(o >= k)(lambda: add(base - 2 * k))
+        pl.when(o + k < outer)(lambda: add(base + 2 * k))
+
+    def take_pair(k):
+        pl.when(o >= k)(lambda: take(1, k, True))
+        pl.when(o + k < outer)(lambda: take(1, k, False))
+        add_pair(k, partner)
+
     step0_partner(1)
     step(1, 1)
+    add(s, True)
+    add(partner)
+    add_pair(1, s)
     for b in range(1, blocks - 1):
         attend_block(b)
     step(1, 2) if outer > 2 else None
@@ -403,23 +427,18 @@
     attend_block(blocks - 1)
     for k in range(3, outer):
         step(1, k)
-    take_all(1)
-
+        take_pair(k - 2)
+        add_pair(k - 1, s)
+    take_pair(outer - 2)
+    add_pair(outer - 1, s)
     step0_partner(2)
-    for n in range(items // tile):
-        rows = pl.ds(n * tile, tile)
-        inner = pl.ds(edge + n * tile, tile)
-        conv_input = project(b_buf, rows, slice(0, cw))
-        before = project(b_buf, rows, slice(2 * cw, 3 * cw))
-        sec[inner, :] = (before * conv_input).astype(bf16)
-        if n == 0:
-            step(2, 1)
+    step(2, 1)
+    take_pair(outer - 1)
+
+    sec[edge : edge + items, :] = (proj[:, 2 * cw :] * proj[:, :cw]).astype(bf16)
     halo(sec, edge, 2)
     if outer > 2:
         step(2, 2)
-    for n in range(items // tile):
-        rows = pl.ds(n * tile, tile)
-        proj[rows, :] = project(b_buf, rows, slice(cw, 2 * cw))
     halo_wait(sec, edge, 2)
     full = sec[...].astype(f32)
     taps = taps_ref[...].astype(f32)
@@ -429,7 +448,7 @@
         + full * taps[1:2]
         + pltpu.roll(full, length - 1, 0) * taps[2:3]
     )
-    mix[:, qw:] = (proj[...] * conv[edge : edge + items]).astype(bf16)
+    mix[:, qw:] = (proj[:, cw : 2 * cw] * conv[edge : edge + items]).astype(bf16)
 
     width = c_buf.shape[2]
 
@@ -544,7 +563,7 @@
         span == 2 * tp and tp % 2 == 0 and depth % 128 == 0 and features == 2 * depth
         and out_attn_weight.shape[1] % 128 == 0 and items % (2 * WINDOW) == 0
         and key_projection.shape[1] == HEAD_SIZE and conv_in_weight.shape[1] % 128 == 0
-        and out_attn_weight.shape[0] == out_conv_weight.shape[0]
+        and out_attn_weight.shape[0] == out_conv_weight.shape[0] and tp > 2
     )
     if not fits:
         return plain_body(
@@ -573,7 +592,7 @@
             pltpu.VMEM((span, mixer, out_attn_weight.shape[1]), bf16),
             pltpu.VMEM((items, qw), bf16),
             pltpu.VMEM((items + 2 * WINDOW, 2 * kw), bf16),
-            pltpu.VMEM((items, cw), f32),
+            pltpu.VMEM((items, 3 * cw), f32),
             pltpu.VMEM((items + 32, cw), bf16),
             pltpu.VMEM((items, mixer), bf16),
             pltpu.VMEM((tp, items, own_width), bf16),

time: 117 us -> 117 us (level)
  no operation moved by 1% of the time
where the time goes in v3:
time: 117 us
  Pallas kernels  113 us (97%)
  local copies, waits for them, and re-layouts  2.06 us (2%)
  other arithmetic  1.63 us (1%)
    pallas_call x1, Pallas kernels, body(): pl.pallas_call(functools.partial(fused_kernel, outer, tp), out_shape=jax....  113 us

profile of v3, /device:TPU:0, one launch (start us, length us, event | category | flops | bytes accessed | tf_op | source)
XLA Modules:
  0.0 116.8 jit_solution(4369469915753010585)
XLA Ops:
  0.0 0.1 pad_maximum_fusion
  0.1 0.7 multiply_sine_fusion.1
  0.8 0.8 multiply_sine_fusion
  1.6 113.0 %shard_map.118 = bf16[768,512]{1,0:T(8,128)(2,1)} custom-call(bf16[768,512]{1,0:T(8,128)(2,1)} %tokens_ref.1, bf16[256,256]{1,0:T(8,128)(2,1)} %wq_ref.1, bf16[256,128]{1,0:T(8,128)(2,1)} %wk_ref.1, bf16[256,128]{1,0:T(8,128)(2,1)} %wv_ref.1, bf16[256,256]{1,0:T(8,128)(2,1)} %wi_ref.1, bf16[256,256]{1,0:T(8,128)(2,1)} %wgo_ref.1, bf16[256,256]{1,0:T(8,128)(2,1)} %wgi_ref.1, ...), custom_call_target="tpu_custom_call" | custom-call | tf_op jit(solution)/shard_map/pallas_call | solution.py:583
  114.7 2.1 %copy.14 = bf16[768,512]{1,0:T(8,128)(2,1)} copy(bf16[768,512]{1,0:T(8,128)(2,1)} %shard_map.118) | data formatting | bytes 1572864
  (3 shorter events, 0.0 us)
